TPU v7x, 32 devices: a whole 2x2x4 slice. The times are simulated.
32 devices in a mesh: grp: 2 (over y), ra: 4 (over z), cb: 4 (over x, core).
Axes of the slice: x: 2, y: 2, z: 4, core: 2. Of those that a mesh axis runs over, the one named last changes fastest.
Arguments:
- residual: bfloat16 [512, 4096], P('grp', 'ra'), parts along dimension 0, may hold values from -6 to 6
- gain_first: bfloat16 [4096], P('ra'), may hold values from 0.099609375 to 1.8984375
- gate_first: bfloat16 [4096, 11264], P('ra', 'cb'), may hold values from -0.09375 to 0.09375
- up_first: bfloat16 [4096, 11264], P('ra', 'cb'), may hold values from -0.09375 to 0.09375
- down_first: bfloat16 [11264, 4096], P('cb', 'ra'), may hold values from -0.078125 to 0.078125
- gain_second: bfloat16 [4096], P('ra'), may hold values from 0.099609375 to 1.8984375
- gate_second: bfloat16 [4096, 11264], P('ra', 'cb'), may hold values from -0.09375 to 0.09375
- up_second: bfloat16 [4096, 11264], P('ra', 'cb'), may hold values from -0.09375 to 0.09375
- down_second: bfloat16 [11264, 4096], P('cb', 'ra'), may hold values from -0.078125 to 0.078125
Outputs:
- updated: bfloat16 [512, 4096], P('grp', 'ra'), parts along dimension 0
There are 2 independent parts, one for each index of `grp`. A program takes and returns all parts, laid end to end along the dimension named above; an argument that names none is the same for every part. Nothing has to cross between parts.
All inputs are finite; a program needn't handle non-finite values.
Results may differ from a plain program's by a relative error of at most 0.0071.
Values may be sent and summed in bfloat16 or wider, within the bound.
A program may use at most 128 MiB of HBM per device.

v0:
```python
import jax
import jax.numpy as jnp
from jax import lax
from jax.sharding import PartitionSpec as P

D = 4096


epsilon = 1e-06


def half_step(stream, gain, w_gate, w_up, w_down):
    values = stream.astype(jnp.float32)
    square_part = jnp.sum(values * values, axis=1, keepdims=True)
    normed = (values * gain.astype(jnp.float32)).astype(jnp.bfloat16)
    gate_part = jnp.dot(normed, w_gate, preferred_element_type=jnp.float32)
    up_part = jnp.dot(normed, w_up, preferred_element_type=jnp.float32)
    gate_sum, up_sum, square_sum = (
        lax.psum_scatter(gate_part, "ra", scatter_dimension=0, tiled=True),
        lax.psum_scatter(up_part, "ra", scatter_dimension=0, tiled=True),
        lax.psum_scatter(square_part, "ra", scatter_dimension=0, tiled=True),
    )
    scale = lax.rsqrt(square_sum / D + epsilon)
    hidden = (jax.nn.silu(scale * gate_sum) * (scale * up_sum)).astype(jnp.bfloat16)
    down_part = jnp.dot(
        lax.all_gather(hidden, "ra", axis=0, tiled=True), w_down, preferred_element_type=jnp.float32
    )
    branch = lax.psum(down_part, "cb")
    return (values + 0.5 * branch).astype(jnp.bfloat16)


def per_device(
    residual,
    gain_first,
    gate_first,
    up_first,
    down_first,
    gain_second,
    gate_second,
    up_second,
    down_second,
):
    middle = half_step(residual, gain_first, gate_first, up_first, down_first)
    return half_step(middle, gain_second, gate_second, up_second, down_second)


def solution(mesh):
    in_specs = (
        P("grp", "ra"),
        P("ra"),
        P("ra", "cb"),
        P("ra", "cb"),
        P("cb", "ra"),
        P("ra"),
        P("ra", "cb"),
        P("ra", "cb"),
        P("cb", "ra"),
    )
    out_specs = P("grp", "ra")
    return jax.shard_map(
        per_device, mesh=mesh, in_specs=in_specs, out_specs=out_specs, check_vma=False
    )
```

profile of v0, /device:TPU:0, one launch (start us, length us, event | category | flops | bytes accessed | tf_op | source)
XLA Modules:
  0.0 450.0 jit_solution(18293002607253876413)
XLA Ops:
  6.5 1.2 fusion
  7.8 0.8 copy.10
  8.6 0.0 reduce-scatter.13.cloned.1.call-start
  8.6 0.7 convert_element_type.31
  9.3 6.1 %fusion.10 = f32[256,2816]{1,0:T(8,128)} fusion(bf16[1024,2816]{1,0:T(8,128)(2,1)} %param.12, bf16[256,1024]{1,0:T(8,128)(2,1)} %param.9, f32[1024]{0:T(1024)S(1)} %convert_element_type.31), kind=kOutput, calls=%fused_computation.16 | convolution fusion | flops 1477181440 | bytes 9179136 | tf_op jit(solution)/shard_map/dot_general | solution.py:17
  15.4 0.0 reduce-scatter.11.cloned.1.call-start
  15.5 5.9 %fusion.12 = f32[256,2816]{1,0:T(8,128)} fusion(bf16[1024,2816]{1,0:T(8,128)(2,1)} %param.11, bf16[256,1024]{1,0:T(8,128)(2,1)S(1)} %copy-done, f32[1024]{0:T(1024)S(1)} %convert_element_type.31), kind=kOutput, calls=%fused_computation.17 | convolution fusion | flops 1477181440 | bytes 9179136 | tf_op jit(solution)/shard_map/dot_general | solution.py:16
  21.5 0.0 all-gather.3.cloned.1.call-start
  21.5 10.3 %reduce-scatter.19.cloned.1.call-done = f32[64,1]{1,0:T(8,128)} async-done(((f32[256,1]{1,0:T(8,128)}), f32[64,1]{1,0:T(8,128)}) %reduce-scatter.19.cloned.1.call-update) | async-done | bytes 272
  31.8 0.8 add_rsqrt_fusion.1
  32.5 0.1 copy.14
  32.6 56.0 %reduce-scatter.13.cloned.1.call-done = f32[64,2816]{1,0:T(8,128)} async-done(((f32[256,2816]{1,0:T(8,128)}), f32[64,2816]{1,0:T(8,128)}) %reduce-scatter.13.cloned.1.call-update) | async-done | bytes 720912 | tf_op jit(solution)/shard_map/reduce_scatter | solution.py:20
  88.6 58.4 %reduce-scatter.11.cloned.1.call-done = f32[64,2816]{1,0:T(8,128)} async-done(((f32[256,2816]{1,0:T(8,128)}), f32[64,2816]{1,0:T(8,128)}) %reduce-scatter.11.cloned.1.call-update) | async-done | bytes 720912 | tf_op jit(solution)/shard_map/reduce_scatter | solution.py:19
  147.0 2.3 multiply_convert_fusion.1
  149.4 34.6 %all-gather.3.cloned.1.call-done = bf16[256,2816]{1,0:T(8,128)(2,1)} async-done(((bf16[64,2816]{1,0:T(8,128)(2,1)}), bf16[256,2816]{1,0:T(8,128)(2,1)}) %all-gather.3.cloned.1.call-update) | async-done | bytes 1441808 | tf_op jit(solution)/shard_map/all_gather | solution.py:26
  184.1 5.7 %fusion.15 = f32[256,1024]{1,0:T(8,128)} fusion(bf16[256,2816]{1,0:T(8,128)(2,1)} %all-gather.3.cloned.1.call-done, bf16[2816,1024]{1,0:T(8,128)(2,1)} %param.13), kind=kOutput, calls=%fused_computation.20 | convolution fusion | flops 1476395008 | bytes 8257536 | tf_op jit(solution)/shard_map/dot_general | solution.py:25
  189.8 35.4 %all-reduce.3.cloned.1.call-done = f32[256,1024]{1,0:T(8,128)} async-done(((f32[256,1024]{1,0:T(8,128)}), f32[256,1024]{1,0:T(8,128)}) %all-reduce.3.cloned.1.call-update) | async-done | bytes 1048592 | tf_op jit(solution)/shard_map/psum | solution.py:28
  225.2 1.5 fusion.3
  226.7 0.8 copy.12
  227.6 5.9 %fusion.8 = f32[256,2816]{1,0:T(8,128)} fusion(bf16[1024,2816]{1,0:T(8,128)(2,1)} %param.15, bf16[256,1024]{1,0:T(8,128)(2,1)S(1)} %get-tuple-element.6, f32[1024]{0:T(1024)S(1)} %convert_element_type.36), kind=kOutput, calls=%fused_computation.15 | convolution fusion | flops 1477181440 | bytes 9179136 | tf_op jit(solution)/shard_map/dot_general | solution.py:16
  233.5 5.9 %fusion.6 = f32[256,2816]{1,0:T(8,128)} fusion(bf16[1024,2816]{1,0:T(8,128)(2,1)} %param.16, bf16[256,1024]{1,0:T(8,128)(2,1)S(1)} %get-tuple-element.6, f32[1024]{0:T(1024)S(1)} %convert_element_type.36), kind=kOutput, calls=%fused_computation.14 | convolution fusion | flops 1477181440 | bytes 9179136 | tf_op jit(solution)/shard_map/dot_general | solution.py:17
  239.6 8.1 %reduce-scatter.21.cloned.1.call-done = f32[64,1]{1,0:T(8,128)} async-done(((f32[256,1]{1,0:T(8,128)}), f32[64,1]{1,0:T(8,128)}) %reduce-scatter.21.cloned.1.call-update) | async-done | bytes 272
  247.6 0.8 add_rsqrt_fusion
  248.4 0.1 copy.15
  248.5 56.0 %reduce-scatter.15.cloned.1.call-done = f32[64,2816]{1,0:T(8,128)} async-done(((f32[256,2816]{1,0:T(8,128)}), f32[64,2816]{1,0:T(8,128)}) %reduce-scatter.15.cloned.1.call-update) | async-done | bytes 720912 | tf_op jit(solution)/shard_map/reduce_scatter | solution.py:19
  304.4 58.4 %reduce-scatter.17.cloned.1.call-done = f32[64,2816]{1,0:T(8,128)} async-done(((f32[256,2816]{1,0:T(8,128)}), f32[64,2816]{1,0:T(8,128)}) %reduce-scatter.17.cloned.1.call-update) | async-done | bytes 720912 | tf_op jit(solution)/shard_map/reduce_scatter | solution.py:20
  362.9 2.3 multiply_convert_fusion
  365.2 0.0 all-reduce.5.cloned.1.call-start
  365.3 34.6 %all-gather.5.cloned.1.call-done = bf16[256,2816]{1,0:T(8,128)(2,1)} async-done(((bf16[64,2816]{1,0:T(8,128)(2,1)}), bf16[256,2816]{1,0:T(8,128)(2,1)}) %all-gather.5.cloned.1.call-update) | async-done | bytes 1441808 | tf_op jit(solution)/shard_map/all_gather | solution.py:26
  399.9 5.7 %fusion.16 = f32[256,1024]{1,0:T(8,128)} fusion(bf16[256,2816]{1,0:T(8,128)(2,1)} %all-gather.5.cloned.1.call-done, bf16[2816,1024]{1,0:T(8,128)(2,1)} %param.17), kind=kOutput, calls=%fused_computation.21 | convolution fusion | flops 1476395008 | bytes 8257536 | tf_op jit(solution)/shard_map/dot_general | solution.py:25
  405.6 35.4 %all-reduce.5.cloned.1.call-done = f32[256,1024]{1,0:T(8,128)} async-done(((f32[256,1024]{1,0:T(8,128)}), f32[256,1024]{1,0:T(8,128)}) %all-reduce.5.cloned.1.call-update) | async-done | bytes 1048592 | tf_op jit(solution)/shard_map/psum | solution.py:28
  441.0 2.2 fusion.5
  (21 shorter events, 0.4 us)
Async XLA Ops:
  6.5 25.2 %reduce-scatter.19.cloned.1.call-start = ((), (), s32[]{:S(2)}) async-start(), calls=%async_computation.14 | async-start | bytes 163840
  8.6 80.0 %reduce-scatter.13.cloned.1.call-start = ((), (), s32[]{:S(2)}) async-start(), calls=%async_computation.7 | async-start | bytes 3604480 | tf_op jit(solution)/shard_map/reduce_scatter | solution.py:20
  9.3 6.2 %copy-start = (bf16[256,1024]{1,0:T(8,128)(2,1)S(1)}, bf16[256,1024]{1,0:T(8,128)(2,1)}, u32[]{:S(2)}) copy-start(bf16[256,1024]{1,0:T(8,128)(2,1)} %param.9) | copy-start | bytes 1572868
  15.4 131.6 %reduce-scatter.11.cloned.1.call-start = ((), (), s32[]{:S(2)}) async-start(), calls=%async_computation.6 | async-start | bytes 3604480 | tf_op jit(solution)/shard_map/reduce_scatter | solution.py:19
  21.5 162.6 %all-gather.3.cloned.1.call-start = ((), (), s32[]{:S(2)}) async-start(), calls=%async_computation.8 | async-start | bytes 1802240 | tf_op jit(solution)/shard_map/all_gather | solution.py:26
  149.4 40.4 %copy-start.1 = (bf16[1024]{0:T(1024)(128)(2,1)S(1)}, bf16[1024]{0:T(1024)(128)(2,1)}, u32[]{:S(2)}) copy-start(bf16[1024]{0:T(1024)(128)(2,1)} %param.14) | copy-start | bytes 6148
  149.4 75.8 %all-reduce.3.cloned.1.call-start = ((), (), s32[]{:S(2)}) async-start(), calls=%async_computation.9 | async-start | bytes 2097152 | tf_op jit(solution)/shard_map/psum | solution.py:28
  189.8 57.9 %reduce-scatter.21.cloned.1.call-start = ((), (), s32[]{:S(2)}) async-start(), calls=%async_computation.15 | async-start | bytes 163840
  227.5 76.9 %reduce-scatter.15.cloned.1.call-start = ((), (), s32[]{:S(2)}) async-start(), calls=%async_computation.10 | async-start | bytes 3604480 | tf_op jit(solution)/shard_map/reduce_scatter | solution.py:19
  233.5 129.4 %reduce-scatter.17.cloned.1.call-start = ((), (), s32[]{:S(2)}) async-start(), calls=%async_computation.11 | async-start | bytes 3604480 | tf_op jit(solution)/shard_map/reduce_scatter | solution.py:20
  239.5 160.4 %all-gather.5.cloned.1.call-start = ((), (), s32[]{:S(2)}) async-start(), calls=%async_computation.12 | async-start | bytes 1802240 | tf_op jit(solution)/shard_map/all_gather | solution.py:26
  365.2 75.8 %all-reduce.5.cloned.1.call-start = ((), (), s32[]{:S(2)}) async-start(), calls=%async_computation.13 | async-start | bytes 2097152 | tf_op jit(solution)/shard_map/psum | solution.py:28
Sparse Core Ops, SparseCore 0:
  9.6 22.1 reduce-scatter.18
  34.1 54.4 reduce-scatter.12
  90.9 56.0 reduce-scatter.10
  149.5 34.5 all-gather.2
  189.9 35.2 all-reduce.2
  227.6 19.9 reduce-scatter.20
  249.9 54.4 reduce-scatter.14
  306.7 56.0 reduce-scatter.16
  365.3 34.5 all-gather.4
  405.7 35.2 all-reduce.4
where the time goes:
time: 451 us; the launch traced here: 450 us
  waiting for transfers between devices  387 us (86%)
  matrix products  35.2 us (8%)
  between operations  13.6 us (3%)
  other arithmetic  11.8 us (3%)
    reduce_scatter x2, waiting for transfers between devices, half_step(): lax.psum_scatter(up_part, 'ra', scatter_dimension=0, tiled=True)  114 us
    reduce_scatter x2, waiting for transfers between devices, half_step(): lax.psum_scatter(gate_part, 'ra', scatter_dimension=0, tiled=True)  114 us
    psum x2, waiting for transfers between devices, half_step(): branch = lax.psum(down_part, 'cb')  70.8 us
    all_gather x2, waiting for transfers between devices, half_step(): lax.all_gather(hidden, 'ra', axis=0, tiled=True)  69.2 us
    unnamed x12, waiting for transfers between devices  18.5 us
    dot_general x2, matrix products, half_step(): up_part = jnp.dot(normed, w_up, preferred_element_type=jnp.float32)  12 us
    dot_general x2, matrix products, half_step(): gate_part = jnp.dot(normed, w_gate, preferred_element_type=jnp.float32)  11.8 us
    dot_general x2, matrix products, half_step(): jnp.dot(lax.all_gather(hidden, 'ra', axis=0, tiled=True), w_down, preferr...  11.4 us
  transfers between devices with their start and end apart: 10, of which 10 were waited for; matrix products, arithmetic and copies ran while one was open for 6% of the time, Pallas kernels for 0%

commit v1 on v0

v1 whole, which is shorter than its diff:
```python
import functools

import jax
import jax.numpy as jnp
from jax import lax
from jax.experimental import pallas as pl
from jax.experimental.pallas import tpu as pltpu
from jax.sharding import PartitionSpec as P

MESH = pl.DeviceIdType.MESH
LANES = 128
epsilon = 1e-06

HOP = 3
REDUCE = 4
SPREAD = 4


def kernel(
    cfg,
    residual,
    gain_first,
    gain_second,
    gate_first,
    up_first,
    down_first,
    gate_second,
    up_second,
    down_second,
    out,
    w_in,
    w_down,
    normed,
    own,
    part_out,
    part_in,
    hidden,
    total,
    rs_own,
    rs_out,
    rs_in,
    merged,
    sq_own,
    sq_out,
    sq_in,
    scale,
    w_sem,
    part_send,
    part_recv,
    hid_send,
    hid_recv,
    sq_send,
    sq_recv,
    rs_send,
    rs_recv,
    ag_send,
    ag_recv,
):
    R, C, blocks, pieces, width, half_rows, gap, model = cfg
    rows = 2 * half_rows
    per_phase = blocks * pieces
    count = 2 * per_phase
    r = lax.axis_index("ra")
    c = lax.axis_index("cb")

    gates, ups, downs = (gate_first, gate_second), (up_first, up_second), (down_first, down_second)

    def weight_copy(phase, p, which):
        span = pl.ds(p * width, width)
        if which == 2:
            return pltpu.make_async_copy(
                downs[phase].at[span, :], w_down.at[phase, p], w_sem.at[phase, 2, p]
            )
        source = (gates, ups)[which][phase]
        return pltpu.make_async_copy(
            source.at[:, span], w_in.at[phase, p, which], w_sem.at[phase, which, p]
        )

    for phase in range(2):
        for p in range(pieces):
            weight_copy(phase, p, 0).start()
            weight_copy(phase, p, 1).start()
        for p in range(pieces):
            weight_copy(phase, p, 2).start()

    barrier = pltpu.get_barrier_semaphore()

    @pl.when(r > 0)
    def _():
        pl.semaphore_signal(barrier, inc=1, device_id={"ra": r - 1}, device_id_type=MESH)

    @pl.when(r < R - 1)
    def _():
        pl.semaphore_signal(barrier, inc=1, device_id={"ra": r + 1}, device_id_type=MESH)

    for k in range(1, C):
        pl.semaphore_signal(
            barrier, inc=1, device_id={"cb": lax.rem(c + k, C)}, device_id_type=MESH
        )

    def prepare(phase, block, stream, gain_ref):
        values = stream.astype(jnp.float32)
        square = jnp.sum(values * values, axis=1, keepdims=True)
        normed[phase, block] = (values * gain_ref[...].astype(jnp.float32)).astype(jnp.bfloat16)
        sq_own[phase, block] = jnp.broadcast_to(square, (rows, LANES)).reshape(2, half_rows, LANES)

    def first(block, carry):
        prepare(0, block, residual[block].reshape(rows, -1), gain_first)
        return carry

    lax.fori_loop(0, blocks, first, 0)

    near = jnp.where(r > 0, 1, 0) + jnp.where(r < R - 1, 1, 0)
    pl.semaphore_wait(barrier, C - 1 + near)

    place = (r, R - 1 - r)
    onward = (r + 1, r - 1)
    back = (r - 1, r + 1)

    def part_copy(d, i):
        return pltpu.make_async_remote_copy(
            src_ref=part_out.at[i, d],
            dst_ref=part_in.at[i, d],
            send_sem=part_send.at[d, i],
            recv_sem=part_recv.at[d, i],
            device_id={"ra": onward[d]},
            device_id_type=MESH,
        )

    def square_copy(d, pb):
        return pltpu.make_async_remote_copy(
            src_ref=sq_out.at[pb, d],
            dst_ref=sq_in.at[pb, d],
            send_sem=sq_send.at[d, pb],
            recv_sem=sq_recv.at[d, pb],
            device_id={"ra": onward[d]},
            device_id_type=MESH,
        )

    def hidden_copy(d, i):
        return pltpu.make_async_remote_copy(
            src_ref=hidden.at[i, d],
            dst_ref=hidden.at[i, d],
            send_sem=hid_send.at[d, i],
            recv_sem=hid_recv.at[d, i],
            device_id={"ra": back[d]},
            device_id_type=MESH,
        )

    def reduce_copy(pb, k):
        peer = lax.rem(c + k, C)
        return pltpu.make_async_remote_copy(
            src_ref=rs_out.at[pb, peer],
            dst_ref=rs_in.at[pb, k - 1],
            send_sem=rs_send.at[pb, k - 1],
            recv_sem=rs_recv.at[pb, k - 1],
            device_id={"cb": peer},
            device_id_type=MESH,
        )

    def spread_copy(pb, k):
        return pltpu.make_async_remote_copy(
            src_ref=merged.at[pb, c],
            dst_ref=merged.at[pb, c],
            send_sem=ag_send.at[pb, k - 1],
            recv_sem=ag_recv.at[pb, k - 1],
            device_id={"cb": lax.rem(c + k, C)},
            device_id_type=MESH,
        )

    def at_step(slot, body):
        early = (slot >= 0) & (slot < per_phase)
        late = (slot >= per_phase + gap) & (slot < count + gap)

        @pl.when(early | late)
        def _():
            phase = jnp.where(late, 1, 0)
            i = slot - phase * gap
            local = i - phase * per_phase
            block = lax.div(local, pieces)
            p = lax.rem(local, pieces)
            body(i, phase, block, p)

    def both_phases(phase, body):
        for static in range(2):

            @pl.when(phase == static)
            def _():
                body(static)

    def project(i, phase, block, p):
        @pl.when(block == 0)
        def _():
            def waits(static):
                weight_copy(static, p, 0).wait()
                weight_copy(static, p, 1).wait()

            both_phases(phase, waits)

        slot = i - phase * per_phase
        x = normed[phase, block]
        for which in range(2):
            product = jnp.dot(x, w_in[phase, p, which], preferred_element_type=jnp.float32)
            own[slot, 0, which] = product[:half_rows]
            own[slot, 1, which] = product[half_rows:]

    def forward(d):
        def body(i, phase, block, p):
            slot = i - phase * per_phase
            pb = phase * blocks + block

            @pl.when(place[d] == 0)
            def _():
                part_out[i, d] = own[slot, d].astype(jnp.bfloat16)
                part_copy(d, i).start()

                @pl.when(p == 0)
                def _():
                    sq_out[pb, d] = sq_own[phase, block, d]
                    square_copy(d, pb).start()

            @pl.when((place[d] > 0) & (place[d] < R - 1))
            def _():
                part_copy(d, i).wait_recv()
                part_out[i, d] = (own[slot, d] + part_in[i, d].astype(jnp.float32)).astype(
                    jnp.bfloat16
                )
                part_copy(d, i).start()

                @pl.when(p == 0)
                def _():
                    square_copy(d, pb).wait_recv()
                    sq_out[pb, d] = sq_own[phase, block, d] + sq_in[pb, d]
                    square_copy(d, pb).start()

            @pl.when(place[d] == R - 1)
            def _():
                @pl.when(p == 0)
                def _():
                    square_copy(d, pb).wait_recv()
                    mean = (sq_own[phase, block, d] + sq_in[pb, d]) / model
                    scale[d] = lax.rsqrt(mean + epsilon)

                part_copy(d, i).wait_recv()
                factor = scale[d][:, :1]
                gate = (own[slot, d, 0] + part_in[i, d, 0].astype(jnp.float32)) * factor
                up = (own[slot, d, 1] + part_in[i, d, 1].astype(jnp.float32)) * factor
                hidden[i, d] = (gate / (1.0 + jnp.exp(-gate)) * up).astype(jnp.bfloat16)
                hidden_copy(d, i).start()

        return body

    def pass_back(d):
        def body(i, phase, block, p):
            @pl.when(place[d] < R - 1)
            def _():
                hidden_copy(d, i).wait_recv()

                @pl.when(place[d] > 0)
                def _():
                    hidden_copy(d, i).start()

        return body

    def down(i, phase, block, p):
        @pl.when(block == 0)
        def _():
            both_phases(phase, lambda static: weight_copy(static, p, 2).wait())

        product = jnp.dot(
            hidden[i].reshape(rows, width), w_down[phase, p], preferred_element_type=jnp.float32
        ).reshape(total.shape)

        @pl.when(p == 0)
        def _():
            total[...] = product

        @pl.when(p > 0)
        def _():
            total[...] += product

        @pl.when(p == pieces - 1)
        def _():
            pb = phase * blocks + block
            rs_own[pb] = total[c]
            rs_out[pb] = total[...].astype(jnp.bfloat16)
            for k in range(1, C):
                reduce_copy(pb, k).start()

    def reduce(i, phase, block, p):
        @pl.when(p == pieces - 1)
        def _():
            pb = phase * blocks + block
            branch = rs_own[pb]
            for k in range(1, C):
                reduce_copy(pb, k).wait_recv()
                branch = branch + rs_in[pb, k - 1].astype(jnp.float32)

            @pl.when(phase == 0)
            def _():
                values = residual[block, c].astype(jnp.float32)
                merged[pb, c] = (values + 0.5 * branch).astype(jnp.bfloat16)

            @pl.when(phase == 1)
            def _():
                values = merged[block, c].astype(jnp.float32)
                merged[pb, c] = (values + 0.5 * branch).astype(jnp.bfloat16)

            for k in range(1, C):
                spread_copy(pb, k).start()

    def spread(i, phase, block, p):
        @pl.when(p == pieces - 1)
        def _():
            pb = phase * blocks + block
            for k in range(1, C):
                spread_copy(pb, k).wait_recv()

            @pl.when(phase == 0)
            def _():
                prepare(1, block, merged[pb].reshape(rows, -1), gain_second)

            @pl.when(phase == 1)
            def _():
                out[block] = merged[pb]

    reach = HOP * (R - 1)
    end = 2 * reach

    def step(s, carry):
        at_step(s - end - REDUCE - SPREAD, spread)
        at_step(s, project)
        for d in range(2):
            at_step(s - HOP * place[d], forward(d))
        for d in range(2):
            at_step(s - reach - HOP * (R - 1 - place[d]), pass_back(d))
        at_step(s - end, down)
        at_step(s - end - REDUCE, reduce)
        return carry

    lax.fori_loop(0, count + gap + end + REDUCE + SPREAD, step, 0)

    def finish(i, carry):
        for d in range(2):

            @pl.when(place[d] < R - 1)
            def _():
                part_copy(d, i).wait_send()

            @pl.when(place[d] > 0)
            def _():
                hidden_copy(d, i).wait_send()

        return carry

    lax.fori_loop(0, count, finish, 0)

    def finish_block(pb, carry):
        for d in range(2):

            @pl.when(place[d] < R - 1)
            def _():
                square_copy(d, pb).wait_send()

        for k in range(1, C):
            reduce_copy(pb, k).wait_send()
            spread_copy(pb, k).wait_send()
        return carry

    lax.fori_loop(0, 2 * blocks, finish_block, 0)


def solution(mesh):
    R, C = mesh.shape["ra"], mesh.shape["cb"]

    def per_device(
        residual,
        gain_first,
        gate_first,
        up_first,
        down_first,
        gain_second,
        gate_second,
        up_second,
        down_second,
    ):
        tokens, depth = residual.shape
        units = gate_first.shape[1]
        blocks = max(1, min(4, tokens // (16 * C)))
        width = 2 * LANES if units % (2 * LANES) == 0 else units
        pieces = units // width
        rows = tokens // blocks
        half_rows = rows // 2
        share = rows // C
        count = 2 * blocks * pieces
        end = 2 * HOP * (R - 1) + REDUCE + SPREAD
        gap = max(0, pieces - 1 + end - blocks * pieces)
        bf16, f32 = jnp.bfloat16, jnp.float32
        vmem = functools.partial(pl.BlockSpec, memory_space=pltpu.VMEM)
        hbm = functools.partial(pl.BlockSpec, memory_space=pl.ANY)
        pbs = 2 * blocks
        dma = pltpu.SemaphoreType.DMA
        result = pl.pallas_call(
            functools.partial(
                kernel, (R, C, blocks, pieces, width, half_rows, gap, float(depth * R))
            ),
            out_shape=jax.ShapeDtypeStruct((blocks, C, share, depth), bf16),
            in_specs=[vmem()] * 3 + [hbm()] * 6,
            out_specs=vmem(),
            scratch_shapes=[
                pltpu.VMEM((2, pieces, 2, depth, width), bf16),
                pltpu.VMEM((2, pieces, width, depth), bf16),
                pltpu.VMEM((2, blocks, rows, depth), bf16),
                pltpu.VMEM((blocks * pieces, 2, 2, half_rows, width), f32),
                pltpu.VMEM((count, 2, 2, half_rows, width), bf16),
                pltpu.VMEM((count, 2, 2, half_rows, width), bf16),
                pltpu.VMEM((count, 2, half_rows, width), bf16),
                pltpu.VMEM((C, share, depth), f32),
                pltpu.VMEM((pbs, share, depth), f32),
                pltpu.VMEM((pbs, C, share, depth), bf16),
                pltpu.VMEM((pbs, C - 1, share, depth), bf16),
                pltpu.VMEM((pbs, C, share, depth), bf16),
                pltpu.VMEM((2, blocks, 2, half_rows, LANES), f32),
                pltpu.VMEM((pbs, 2, half_rows, LANES), f32),
                pltpu.VMEM((pbs, 2, half_rows, LANES), f32),
                pltpu.VMEM((2, half_rows, LANES), f32),
                dma((2, 3, pieces)),
                dma((2, count)),
                dma((2, count)),
                dma((2, count)),
                dma((2, count)),
                dma((2, pbs)),
                dma((2, pbs)),
                dma((pbs, C - 1)),
                dma((pbs, C - 1)),
                dma((pbs, C - 1)),
                dma((pbs, C - 1)),
            ],
            compiler_params=pltpu.CompilerParams(
                collective_id=0, has_side_effects=True, vmem_limit_bytes=67043328
            ),
        )(
            residual.reshape(blocks, C, share, depth),
            gain_first.reshape(1, depth),
            gain_second.reshape(1, depth),
            gate_first,
            up_first,
            down_first,
            gate_second,
            up_second,
            down_second,
        )
        return result.reshape(tokens, depth)

    in_specs = (
        P("grp", "ra"),
        P("ra"),
        P("ra", "cb"),
        P("ra", "cb"),
        P("cb", "ra"),
        P("ra"),
        P("ra", "cb"),
        P("ra", "cb"),
        P("cb", "ra"),
    )
    return jax.shard_map(
        per_device, mesh=mesh, in_specs=in_specs, out_specs=P("grp", "ra"), check_vma=False
    )
```

time: 451 us -> 142 us (0.31)
  waiting for transfers between devices: 387 us -> 0 us
  Pallas kernels: 0 us -> 137 us
  matrix products: 35.2 us -> 0 us
  between operations: 13.6 us -> 0.01 us
  other arithmetic: 11.8 us -> 0 us
    reduce_scatter x4 -> x0, waiting for transfers between devices: 229 us -> none  [the longest x2 114 us: half_step(): lax.psum_scatter(up_part, 'ra', scatter_dimension=0, tiled=True)]
    pallas_call x0 -> x1, Pallas kernels: none -> 137 us  [per_device(): pl.pallas_call(functools.partial(kernel, (R, C, blocks, pieces, width, ha...]
    psum x2 -> x0, waiting for transfers between devices: 70.8 us -> none  [half_step(): branch = lax.psum(down_part, 'cb')]
    all_gather x2 -> x0, waiting for transfers between devices: 69.2 us -> none  [half_step(): lax.all_gather(hidden, 'ra', axis=0, tiled=True)]
    dot_general x6 -> x0, matrix products: 35.2 us -> none  [the longest x2 12 us: half_step(): up_part = jnp.dot(normed, w_up, preferred_element_type=jnp.float32)]
    unnamed x12 -> x0, waiting for transfers between devices: 18.5 us -> none
    convert_element_type x5 -> x0, other arithmetic: 7.54 us -> none  [the longest x2 4.68 us: half_step(): (jax.nn.silu(scale * gate_sum) * (scale * up_sum)).astype(jnp.bfloat16)]
  transfers between devices with their start and end apart: 10 -> 0, of which waited for: 10 -> 0; matrix products, arithmetic and copies ran while one was open for 6% -> 0% of each run, Pallas kernels for 0% -> 0%
where the time goes in v1:
time: 142 us; the launch traced here: 141 us
  Pallas kernels  137 us (96%)
  local copies, waits for them, and re-layouts  4.42 us (3%)
    pallas_call x1, Pallas kernels, per_device(): pl.pallas_call(functools.partial(kernel, (R, C, blocks, pieces, width, ha...  137 us

profile of v1, /device:TPU:0, one launch (start us, length us, event | category | flops | bytes accessed | tf_op | source)
XLA Modules:
  0.0 141.3 jit_solution(13437296019423739009)
XLA Ops:
  0.0 1.3 reshape.13.gain_first
  1.3 1.3 reshape.14.gain_second
  2.6 136.9 %shard_map.91 = bf16[4,4,16,1024]{3,2,1,0:T(8,128)(2,1)} custom-call(bf16[4,4,16,1024]{3,2,1,0:T(8,128)(2,1)} %bitcast.3, bf16[1,1024]{1,0:T(2,128)(2,1)} %reshape.13.gain_first, bf16[1,1024]{1,0:T(2,128)(2,1)} %reshape.14.gain_second, bf16[1024,2816]{1,0:T(8,128)(2,1)} %gate_first.1, bf16[1024,2816]{1,0:T(8,128)(2,1)} %up_first.1, ...), custom_call_target="tpu_custom_call" | custom-call | tf_op jit(solution)/shard_map/pallas_call | solution.py:403
  139.4 1.9 %copy.11 = bf16[256,1024]{1,0:T(8,128)(2,1)} copy(bf16[256,1024]{1,0:T(8,128)(2,1)} %bitcast.2) | data formatting | bytes 1048576

commit v2 on v1

--- a/solution.py
+++ b/solution.py
@@ -11,9 +11,10 @@
 LANES = 128
 epsilon = 1e-06
 
-HOP = 3
+HOP = 4
 REDUCE = 4
 SPREAD = 4
+TILE = 8
 
 
 def kernel(
@@ -76,12 +77,23 @@
             source.at[:, span], w_in.at[phase, p, which], w_sem.at[phase, which, p]
         )
 
-    for phase in range(2):
-        for p in range(pieces):
-            weight_copy(phase, p, 0).start()
-            weight_copy(phase, p, 1).start()
-        for p in range(pieces):
-            weight_copy(phase, p, 2).start()
+    for p in range(pieces):
+        weight_copy(0, p, 0).start()
+        weight_copy(0, p, 1).start()
+
+    def load_rest(s):
+        @pl.when(s == 2)
+        def _():
+            for p in range(pieces):
+                weight_copy(0, p, 2).start()
+
+        @pl.when(s == 6)
+        def _():
+            for p in range(pieces):
+                weight_copy(1, p, 0).start()
+                weight_copy(1, p, 1).start()
+            for p in range(pieces):
+                weight_copy(1, p, 2).start()
 
     barrier = pltpu.get_barrier_semaphore()
 
@@ -97,18 +109,24 @@
         pl.semaphore_signal(
             barrier, inc=1, device_id={"cb": lax.rem(c + k, C)}, device_id_type=MESH
         )
+
+    def diagonal():
+        shape = (half_rows, half_rows)
+        return lax.broadcasted_iota(jnp.int32, shape, 0) == lax.broadcasted_iota(jnp.int32, shape, 1)
 
     def prepare(phase, block, stream, gain_ref):
         values = stream.astype(jnp.float32)
         square = jnp.sum(values * values, axis=1, keepdims=True)
         normed[phase, block] = (values * gain_ref[...].astype(jnp.float32)).astype(jnp.bfloat16)
-        sq_own[phase, block] = jnp.broadcast_to(square, (rows, LANES)).reshape(2, half_rows, LANES)
-
-    def first(block, carry):
+        for d in range(2):
+            column = square[d * half_rows : (d + 1) * half_rows]
+            line = jnp.sum(jnp.where(diagonal(), column, 0.0), axis=0, keepdims=True)
+            sq_own[phase, block, d] = jnp.broadcast_to(line, (TILE, half_rows))
+
+    def first(block):
         prepare(0, block, residual[block].reshape(rows, -1), gain_first)
-        return carry
-
-    lax.fori_loop(0, blocks, first, 0)
+
+    first(0)
 
     near = jnp.where(r > 0, 1, 0) + jnp.where(r < R - 1, 1, 0)
     pl.semaphore_wait(barrier, C - 1 + near)
@@ -238,8 +256,10 @@
                 @pl.when(p == 0)
                 def _():
                     square_copy(d, pb).wait_recv()
-                    mean = (sq_own[phase, block, d] + sq_in[pb, d]) / model
-                    scale[d] = lax.rsqrt(mean + epsilon)
+                    mean = (sq_own[phase, block, d] + sq_in[pb, d])[:1] / model
+                    line = lax.rsqrt(mean + epsilon)
+                    column = jnp.sum(jnp.where(diagonal(), line, 0.0), axis=1, keepdims=True)
+                    scale[d] = jnp.broadcast_to(column, (half_rows, LANES))
 
                 part_copy(d, i).wait_recv()
                 factor = scale[d][:, :1]
@@ -328,17 +348,23 @@
     end = 2 * reach
 
     def step(s, carry):
-        at_step(s - end - REDUCE - SPREAD, spread)
+        load_rest(s)
+        for d in range(2):
+            at_step(s - 1 - HOP * place[d], forward(d))
+        for d in range(2):
+            at_step(s - 1 - reach - HOP * (R - 1 - place[d]), pass_back(d))
+        at_step(s - 1 - end, down)
+        at_step(s - 1 - end - REDUCE, reduce)
+        at_step(s - 1 - end - REDUCE - SPREAD, spread)
+
+        @pl.when(s + 1 < blocks)
+        def _():
+            first(s + 1)
+
         at_step(s, project)
-        for d in range(2):
-            at_step(s - HOP * place[d], forward(d))
-        for d in range(2):
-            at_step(s - reach - HOP * (R - 1 - place[d]), pass_back(d))
-        at_step(s - end, down)
-        at_step(s - end - REDUCE, reduce)
         return carry
 
-    lax.fori_loop(0, count + gap + end + REDUCE + SPREAD, step, 0)
+    lax.fori_loop(0, count + gap + end + REDUCE + SPREAD + 1, step, 0)
 
     def finish(i, carry):
         for d in range(2):
@@ -393,7 +419,7 @@
         half_rows = rows // 2
         share = rows // C
         count = 2 * blocks * pieces
-        end = 2 * HOP * (R - 1) + REDUCE + SPREAD
+        end = 1 + 2 * HOP * (R - 1) + REDUCE + SPREAD
         gap = max(0, pieces - 1 + end - blocks * pieces)
         bf16, f32 = jnp.bfloat16, jnp.float32
         vmem = functools.partial(pl.BlockSpec, memory_space=pltpu.VMEM)
@@ -420,9 +446,9 @@
                 pltpu.VMEM((pbs, C, share, depth), bf16),
                 pltpu.VMEM((pbs, C - 1, share, depth), bf16),
                 pltpu.VMEM((pbs, C, share, depth), bf16),
-                pltpu.VMEM((2, blocks, 2, half_rows, LANES), f32),
-                pltpu.VMEM((pbs, 2, half_rows, LANES), f32),
-                pltpu.VMEM((pbs, 2, half_rows, LANES), f32),
+                pltpu.VMEM((2, blocks, 2, TILE, half_rows), f32),
+                pltpu.VMEM((pbs, 2, TILE, half_rows), f32),
+                pltpu.VMEM((pbs, 2, TILE, half_rows), f32),
                 pltpu.VMEM((2, half_rows, LANES), f32),
                 dma((2, 3, pieces)),
                 dma((2, count)),

time: 142 us -> 135 us (0.951)
  Pallas kernels: 137 us -> 130 us
    pallas_call x1, Pallas kernels: 137 us -> 130 us  [per_device(): pl.pallas_call(functools.partial(kernel, (R, C, blocks, pieces, width, ha...]
where the time goes in v2:
time: 135 us; the launch traced here: 134 us
  Pallas kernels  130 us (96%)
  local copies, waits for them, and re-layouts  4.42 us (3%)
    pallas_call x1, Pallas kernels, per_device(): pl.pallas_call(functools.partial(kernel, (R, C, blocks, pieces, width, ha...  130 us

profile of v2, /device:TPU:0, one launch (start us, length us, event | category | flops | bytes accessed | tf_op | source)
XLA Modules:
  0.0 134.3 jit_solution(11253158300435703291)
XLA Ops:
  0.0 1.3 reshape.13.gain_first
  1.3 1.3 reshape.14.gain_second
  2.6 129.9 %shard_map.91 = bf16[4,4,16,1024]{3,2,1,0:T(8,128)(2,1)} custom-call(bf16[4,4,16,1024]{3,2,1,0:T(8,128)(2,1)} %bitcast.3, bf16[1,1024]{1,0:T(2,128)(2,1)} %reshape.13.gain_first, bf16[1,1024]{1,0:T(2,128)(2,1)} %reshape.14.gain_second, bf16[1024,2816]{1,0:T(8,128)(2,1)} %gate_first.1, bf16[1024,2816]{1,0:T(8,128)(2,1)} %up_first.1, ...), custom_call_target="tpu_custom_call" | custom-call | tf_op jit(solution)/shard_map/pallas_call | solution.py:429
  132.4 1.9 %copy.11 = bf16[256,1024]{1,0:T(8,128)(2,1)} copy(bf16[256,1024]{1,0:T(8,128)(2,1)} %bitcast.2) | data formatting | bytes 1048576
